TPU v7x, 128 devices: a whole 4x4x4 slice. The times are simulated.
128 devices in a mesh: fs: 16 (over z, y), tp: 8 (over x, core).
Axes of the slice: x: 4, y: 4, z: 4, core: 2. Of those that a mesh axis runs over, the one named last changes fastest.
Arguments:
- tokens: bfloat16 [16, 384, 2048], P('fs', None, 'tp'), may hold values from -16 to 16
- first_gate: bfloat16 [2048, 6144], P('fs', 'tp'), may hold values from -0.125 to 0.125
- first_up: bfloat16 [2048, 6144], P('fs', 'tp'), may hold values from -0.125 to 0.125
- first_down: bfloat16 [6144, 2048], P('tp', 'fs'), may hold values from -0.078125 to 0.078125
- first_gain: bfloat16 [2048], P('tp'), may hold values from 0.099609375 to 1.8984375
- glu_value: bfloat16 [2048, 1024], P('fs', 'tp'), may hold values from -0.125 to 0.125
- glu_gate: bfloat16 [2048, 1024], P('fs', 'tp'), may hold values from -0.125 to 0.125
- conv_taps: bfloat16 [31, 1024], P(None, 'tp'), may hold values from -3 to 3
- conv_gain: bfloat16 [1024], P('tp'), may hold values from 0.099609375 to 1.8984375
- conv_proj: bfloat16 [1024, 2048], P('tp', 'fs'), may hold values from -0.1875 to 0.1875
- second_gain: bfloat16 [2048], P('tp'), may hold values from 0.099609375 to 1.8984375
- last_gate: bfloat16 [2048, 6144], P('fs', 'tp'), may hold values from -0.125 to 0.125
- last_up: bfloat16 [2048, 6144], P('fs', 'tp'), may hold values from -0.125 to 0.125
- last_down: bfloat16 [6144, 2048], P('tp', 'fs'), may hold values from -0.078125 to 0.078125
- third_gain: bfloat16 [2048], P('tp'), may hold values from 0.099609375 to 1.8984375
Outputs:
- layer_out: bfloat16 [16, 384, 2048], P('fs', None, 'tp')
All inputs are finite; a program needn't handle non-finite values.
Results may differ from a plain program's by a relative error of at most 0.015.
Values may be sent and summed in bfloat16 or wider, within the bound.
No kernel may reach another device: no remote copies, remote signals or barrier semaphores. Data moves between devices by JAX's collectives and lax.ppermute only.
A program may use at most 64 MiB of HBM per device.

v0:
```python
import jax
import jax.numpy as jnp
from jax import lax
from jax.sharding import PartitionSpec as P

ALPHA = 2.0**0.25
EPSILON = 1e-05


def sent_to_all(value, axis):
    copies = jnp.broadcast_to(value, (lax.axis_size(axis), *value.shape))
    return lax.all_to_all(copies, axis, split_axis=0, concat_axis=0, tiled=True)


def over_copies(value, axis):
    everything = sent_to_all(value, axis)
    return jnp.sum(everything, axis=0)


def in_one(arrays, axis):
    ravelled, at, gathered = (jnp.concatenate([a.reshape(-1) for a in arrays]), 0, [])
    running = over_copies(ravelled, axis)
    for a in arrays:
        gathered.append(running[at : at + a.size].reshape(a.shape))
        at += a.size
    return tuple(gathered)


def laid_out(blocks, dim):
    lengths = list(blocks.shape[1:])
    lengths[dim] *= blocks.shape[0]
    return jnp.moveaxis(blocks, 0, dim).reshape(lengths)


def gathered_copies(value, axis, dim):
    return laid_out(sent_to_all(value, axis), dim)


def cut_along(value, dim, peers):
    before, after = (value.shape[:dim], value.shape[dim + 1 :])
    return jnp.moveaxis(value.reshape(*before, peers, -1, *after), dim, 0)


def sent_and_summed(value, axis, dim):
    blocks = cut_along(value, dim, lax.axis_size(axis))
    arrived = lax.all_to_all(blocks, axis, split_axis=0, concat_axis=0, tiled=True)
    return arrived.astype(jnp.float32).sum(axis=0)


def sent_together(arrays, axis, dim, along):
    widths = [a.shape[along] for a in arrays]
    both = jnp.concatenate(arrays, axis=along)
    out = lax.all_gather(both, axis, axis=dim, tiled=True)
    return tuple(jnp.split(out, [sum(widths[:k]) for k in range(1, len(widths))], axis=along))


def norm_split(values, gain):
    width_all = values.shape[-1] * lax.axis_size("tp")
    sums, squares = in_one(
        (jnp.sum(values, axis=-1, keepdims=True), jnp.sum(values * values, axis=-1, keepdims=True)),
        "tp",
    )
    center = sums / width_all
    spread = squares / width_all - center * center
    return (values - center) * lax.rsqrt(spread + EPSILON) * gain.astype(jnp.float32)


def gather_features(current):
    return gathered_copies(current, "tp", 1)


def scatter_rows(partial_value):
    return sent_and_summed(partial_value.astype(jnp.bfloat16), "tp", 1)


def fold_rows(gathered, shard_rows):
    return (
        jnp.dot(gathered, shard_rows[0], preferred_element_type=jnp.float32),
        jnp.dot(gathered, shard_rows[1], preferred_element_type=jnp.float32),
    )


def feed_forward(current, w_gate, w_up, w_down):
    full_down = lax.all_gather(w_down, "fs", axis=1, tiled=True)
    gathered = gather_features(current)
    gate, upward = fold_rows(gathered, sent_together((w_gate, w_up), "fs", 0, 1))
    hidden = (jax.nn.silu(gate) * upward).astype(jnp.bfloat16)
    partial_value = jnp.dot(hidden, full_down, preferred_element_type=jnp.float32)
    return scatter_rows(partial_value)


def conv_module(current, glu_value, glu_gate, conv_taps, conv_gain, conv_proj):
    gathered = gather_features(current)
    value, gate = fold_rows(gathered, sent_together((glu_value, glu_gate), "fs", 0, 1))
    gated = value * jax.nn.sigmoid(gate)
    reach = (conv_taps.shape[0] - 1) // 2
    length = gated.shape[0]
    padded = jnp.pad(gated, ((reach, reach), (0, 0)))
    taps = conv_taps.astype(jnp.float32)
    mixed = jnp.zeros_like(gated)
    for tap_index in range(conv_taps.shape[0]):
        mixed = mixed + taps[tap_index] * padded[tap_index : tap_index + length]
    normed = jax.nn.silu(norm_split(mixed, conv_gain)).astype(jnp.bfloat16)
    partial_value = jnp.dot(
        normed, gathered_copies(conv_proj, "fs", 1), preferred_element_type=jnp.float32
    )
    return scatter_rows(partial_value)


def post_norm(current, branch, weight, gain):
    mixed = ALPHA * current.astype(jnp.float32) + weight * branch
    return norm_split(mixed, gain).astype(jnp.bfloat16)


def body(
    tokens,
    first_gate,
    first_up,
    first_down,
    first_gain,
    glu_value,
    glu_gate,
    conv_taps,
    conv_gain,
    conv_proj,
    second_gain,
    last_gate,
    last_up,
    last_down,
    third_gain,
):
    current = tokens[0]
    first = post_norm(
        current, feed_forward(current, first_gate, first_up, first_down), 0.5, first_gain
    )
    second = post_norm(
        first,
        conv_module(first, glu_value, glu_gate, conv_taps, conv_gain, conv_proj),
        1.0,
        second_gain,
    )
    output = post_norm(second, feed_forward(second, last_gate, last_up, last_down), 0.5, third_gain)
    return output[None]


def solution(mesh):
    return jax.shard_map(
        body,
        mesh=mesh,
        in_specs=(
            P("fs", None, "tp"),
            P("fs", "tp"),
            P("fs", "tp"),
            P("tp", "fs"),
            P("tp"),
            P("fs", "tp"),
            P("fs", "tp"),
            P(None, "tp"),
            P("tp"),
            P("tp", "fs"),
            P("tp"),
            P("fs", "tp"),
            P("fs", "tp"),
            P("tp", "fs"),
            P("tp"),
        ),
        out_specs=P("fs", None, "tp"),
        check_vma=False,
    )
```

profile of v0, /device:TPU:1, one launch (start us, length us, event | category | flops | bytes accessed | tf_op | source)
XLA Modules:
  0.0 349.3 jit_solution(4812585202268333677)
XLA Ops:
  6.5 1.9 pad_maximum_fusion
  8.5 0.7 all-gather.8.cloned.1.call-update
  9.2 1.4 pad_maximum_fusion.2
  10.7 0.8 pad_maximum_fusion.1
  11.9 26.1 %all_to_all.59 = bf16[8,384,256]{1,2,0:T(8,128)(2,1)S(1)} all-to-all(bf16[8,384,256]{1,2,0:T(8,128)(2,1)S(1)} %broadcast_in_dim.29), channel_id=1, replica_groups=mesh['fs'=16,'tp'=8] {'tp'}, dimensions={0} | all-to-all | bytes 3145728 | tf_op jit(solution)/shard_map/all_to_all | solution.py:12
  38.0 35.9 %all-gather.6.cloned.1.call-done = bf16[2048,1536]{1,0:T(8,128)(2,1)} async-done(((bf16[128,1536]{1,0:T(8,128)(2,1)}), bf16[2048,1536]{1,0:T(8,128)(2,1)}) %all-gather.6.cloned.1.call-update) | async-done | bytes 6291472 | tf_op jit(solution)/shard_map/all_gather | solution.py:53
  73.9 4.7 %fusion.8 = f32[384,768]{0,1:T(8,128)} fusion(bf16[384,2048]{0,1:T(8,128)(2,1)S(1)} %bitcast.164, bf16[2048,1536]{1,0:T(8,128)(2,1)} %all-gather.6.cloned.1.call-done), kind=kOutput, calls=%fused_computation.17 | convolution fusion | flops 1207959552 | bytes 5898240 | tf_op jit(solution)/shard_map/dot_general | solution.py:78
  78.6 47.8 %all-gather.8.cloned.1.call-done = bf16[768,2048]{1,0:T(8,128)(2,1)} async-done(((bf16[768,128]{1,0:T(8,128)(2,1)}), bf16[768,2048]{1,0:T(8,128)(2,1)}) %all-gather.8.cloned.1.call-update) | async-done | bytes 3145744 | tf_op jit(solution)/shard_map/all_gather | solution.py:84
  126.4 6.3 %convolution_convert_fusion.1 = bf16[384,2048]{1,0:T(8,128)(2,1)S(1)} fusion(bf16[768,2048]{1,0:T(8,128)(2,1)} %all-gather.8.cloned.1.call-done, bf16[384,2048]{0,1:T(8,128)(2,1)S(1)} %bitcast.165, bf16[2048,1536]{1,0:T(8,128)(2,1)} %all-gather.6.cloned.1.call-done, f32[384,768]{0,1:T(8,128)} %fusion.8), kind=kOutput, calls=%fused_computation.12 | convolution fusion | flops 2418475008 | bytes 10616832 | tf_op jit(solution)/shard_map/dot_general | solution.py:88
  132.9 26.6 %all_to_all.60 = bf16[8,384,256]{2,1,0:T(8,128)(2,1)S(1)} all-to-all(bf16[8,384,256]{2,1,0:T(8,128)(2,1)S(1)} %bitcast.155), channel_id=1, replica_groups=mesh['fs'=16,'tp'=8] {'tp'}, dimensions={0} | all-to-all | bytes 3145728 | tf_op jit(solution)/shard_map/all_to_all | solution.py:46
  159.5 0.2 convert_reduce_fusion.2
  159.7 0.2 fusion.84
  159.9 0.6 broadcast_in_dim.30
  160.6 4.3 %all-to-all-start.2 = ((f32[8,1,768]{2,1,0:T(1,128)}), f32[8,1,768]{2,1,0:T(1,128)S(1)}, u32[]{:S(2)}, u32[]{:S(2)}) async-start(f32[8,1,768]{2,1,0:T(1,128)} %broadcast_in_dim.30), calls=%async_computation.2 | async-start | bytes 49152 | tf_op jit(solution)/shard_map/all_to_all | solution.py:12
  164.8 4.7 %all-to-all-done.2 = f32[8,1,768]{2,1,0:T(1,128)S(1)} async-done(((f32[8,1,768]{2,1,0:T(1,128)}), f32[8,1,768]{2,1,0:T(1,128)S(1)}, u32[]{:S(2)}, u32[]{:S(2)}) %all-to-all-start.2) | async-done | bytes 24608 | tf_op jit(solution)/shard_map/all_to_all | solution.py:12
  169.9 1.3 broadcast_in_dim.31
  171.2 4.3 %all-to-all-start.3 = ((bf16[8,384,256]{1,2,0:T(8,128)(2,1)}), bf16[8,384,256]{1,2,0:T(8,128)(2,1)S(1)}, u32[]{:S(2)}, u32[]{:S(2)}) async-start(bf16[8,384,256]{1,2,0:T(8,128)(2,1)} %broadcast_in_dim.31), calls=%async_computation.3 | async-start | bytes 3145728 | tf_op jit(solution)/shard_map/all_to_all | solution.py:12
  175.6 0.6 all-gather.14.cloned.1.call-update
  176.2 20.0 %all-to-all-done.3 = bf16[8,384,256]{1,2,0:T(8,128)(2,1)S(1)} async-done(((bf16[8,384,256]{1,2,0:T(8,128)(2,1)}), bf16[8,384,256]{1,2,0:T(8,128)(2,1)S(1)}, u32[]{:S(2)}, u32[]{:S(2)}) %all-to-all-start.3) | async-done | bytes 1572896 | tf_op jit(solution)/shard_map/all_to_all | solution.py:12
  196.2 1.7 fusion.37
  198.0 0.6 fusion.29
  198.6 0.8 fusion.88
  199.4 0.6 broadcast_in_dim.32
  200.0 4.2 %all-to-all-start.4 = ((f32[8,1,768]{2,1,0:T(1,128)}), f32[8,1,768]{2,1,0:T(1,128)S(1)}, u32[]{:S(2)}, u32[]{:S(2)}) async-start(f32[8,1,768]{2,1,0:T(1,128)} %broadcast_in_dim.32), calls=%async_computation.4 | async-start | bytes 49152 | tf_op jit(solution)/shard_map/all_to_all | solution.py:12
  204.3 4.6 %all-to-all-done.4 = f32[8,1,768]{2,1,0:T(1,128)S(1)} async-done(((f32[8,1,768]{2,1,0:T(1,128)}), f32[8,1,768]{2,1,0:T(1,128)S(1)}, u32[]{:S(2)}, u32[]{:S(2)}) %all-to-all-start.4) | async-done | bytes 24608 | tf_op jit(solution)/shard_map/all_to_all | solution.py:12
  208.9 0.9 broadcast_in_dim.33
  209.8 4.7 %all-to-all-start.5 = ((bf16[16,128,128]{1,2,0:T(8,128)(2,1)}), bf16[16,128,128]{1,2,0:T(8,128)(2,1)S(1)}, u32[]{:S(2)}, u32[]{:S(2)}) async-start(bf16[16,128,128]{1,2,0:T(8,128)(2,1)} %broadcast_in_dim.33), calls=%async_computation.5 | async-start | bytes 1048576 | tf_op jit(solution)/shard_map/all_to_all | solution.py:12
  214.6 17.0 %all-to-all-done.5 = bf16[16,128,128]{1,2,0:T(8,128)(2,1)S(1)} async-done(((bf16[16,128,128]{1,2,0:T(8,128)(2,1)}), bf16[16,128,128]{1,2,0:T(8,128)(2,1)S(1)}, u32[]{:S(2)}, u32[]{:S(2)}) %all-to-all-start.5) | async-done | bytes 524320 | tf_op jit(solution)/shard_map/all_to_all | solution.py:12
  231.6 0.6 convolution_convert_fusion.2
  232.3 25.0 %all_to_all.61 = bf16[8,384,256]{2,1,0:T(8,128)(2,1)S(1)} all-to-all(bf16[8,384,256]{2,1,0:T(8,128)(2,1)S(1)} %bitcast.156), channel_id=1, replica_groups=mesh['fs'=16,'tp'=8] {'tp'}, dimensions={0} | all-to-all | bytes 3145728 | tf_op jit(solution)/shard_map/all_to_all | solution.py:46
  257.3 0.2 convert_reduce_fusion.1
  257.5 0.2 fusion.79
  257.8 0.6 broadcast_in_dim.34
  258.4 4.3 %all-to-all-start.7 = ((f32[8,1,768]{2,1,0:T(1,128)}), f32[8,1,768]{2,1,0:T(1,128)S(1)}, u32[]{:S(2)}, u32[]{:S(2)}) async-start(f32[8,1,768]{2,1,0:T(1,128)} %broadcast_in_dim.34), calls=%async_computation.7 | async-start | bytes 49152 | tf_op jit(solution)/shard_map/all_to_all | solution.py:12
  262.7 4.7 %all-to-all-done.7 = f32[8,1,768]{2,1,0:T(1,128)S(1)} async-done(((f32[8,1,768]{2,1,0:T(1,128)}), f32[8,1,768]{2,1,0:T(1,128)S(1)}, u32[]{:S(2)}, u32[]{:S(2)}) %all-to-all-start.7) | async-done | bytes 24608 | tf_op jit(solution)/shard_map/all_to_all | solution.py:12
  267.8 1.3 broadcast_in_dim.35
  269.1 4.2 %all-to-all-start.8 = ((bf16[8,384,256]{1,2,0:T(8,128)(2,1)}), bf16[8,384,256]{1,2,0:T(8,128)(2,1)S(1)}, u32[]{:S(2)}, u32[]{:S(2)}) async-start(bf16[8,384,256]{1,2,0:T(8,128)(2,1)} %broadcast_in_dim.35), calls=%async_computation.8 | async-start | bytes 3145728 | tf_op jit(solution)/shard_map/all_to_all | solution.py:12
  273.3 20.6 %all-to-all-done.8 = bf16[8,384,256]{1,2,0:T(8,128)(2,1)S(1)} async-done(((bf16[8,384,256]{1,2,0:T(8,128)(2,1)}), bf16[8,384,256]{1,2,0:T(8,128)(2,1)S(1)}, u32[]{:S(2)}, u32[]{:S(2)}) %all-to-all-start.8) | async-done | bytes 1572896 | tf_op jit(solution)/shard_map/all_to_all | solution.py:12
  293.9 4.8 %fusion.2 = f32[384,768]{0,1:T(8,128)} fusion(bf16[384,2048]{0,1:T(8,128)(2,1)S(1)} %bitcast.162, bf16[2048,1536]{1,0:T(8,128)(2,1)} %all-gather.12.cloned.1.call-done), kind=kOutput, calls=%fused_computation.2 | convolution fusion | flops 1207959552 | bytes 5898240 | tf_op jit(solution)/shard_map/dot_general | solution.py:78
  298.6 7.6 %convolution_convert_fusion = bf16[384,2048]{1,0:T(8,128)(2,1)} fusion(bf16[768,2048]{1,0:T(8,128)(2,1)} %all-gather.14.cloned.1.call-done, bf16[384,2048]{0,1:T(8,128)(2,1)S(1)} %bitcast.163, bf16[2048,1536]{1,0:T(8,128)(2,1)} %all-gather.12.cloned.1.call-done, f32[384,768]{0,1:T(8,128)} %fusion.2), kind=kOutput, calls=%fused_computation.11 | convolution fusion | flops 2418475008 | bytes 10616832 | tf_op jit(solution)/shard_map/dot_general | solution.py:88
  306.2 1.5 copy.78
  307.7 23.9 %all_to_all.62 = bf16[8,384,256]{2,1,0:T(8,128)(2,1)S(1)} all-to-all(bf16[8,384,256]{2,1,0:T(8,128)(2,1)S(1)} %bitcast.157), channel_id=1, replica_groups=mesh['fs'=16,'tp'=8] {'tp'}, dimensions={0} | all-to-all | bytes 3145728 | tf_op jit(solution)/shard_map/all_to_all | solution.py:46
  331.7 0.2 convert_reduce_fusion
  331.9 0.2 fusion.51
  332.1 0.6 broadcast_in_dim.36
  332.7 4.3 %all-to-all-start.10 = ((f32[8,1,768]{2,1,0:T(1,128)}), f32[8,1,768]{2,1,0:T(1,128)S(1)}, u32[]{:S(2)}, u32[]{:S(2)}) async-start(f32[8,1,768]{2,1,0:T(1,128)} %broadcast_in_dim.36), calls=%async_computation.10 | async-start | bytes 49152 | tf_op jit(solution)/shard_map/all_to_all | solution.py:12
  337.0 4.7 %all-to-all-done.10 = f32[8,1,768]{2,1,0:T(1,128)S(1)} async-done(((f32[8,1,768]{2,1,0:T(1,128)}), f32[8,1,768]{2,1,0:T(1,128)S(1)}, u32[]{:S(2)}, u32[]{:S(2)}) %all-to-all-start.10) | async-done | bytes 24608 | tf_op jit(solution)/shard_map/all_to_all | solution.py:12
  341.7 1.1 fusion.42
  (59 shorter events, 1.8 us)
Async XLA Ops:
  6.5 4.2 %copy-start.2 = (bf16[128,768]{1,0:T(8,128)(2,1)S(1)}, bf16[128,768]{1,0:T(8,128)(2,1)}, u32[]{:S(2)}) copy-start(bf16[128,768]{1,0:T(8,128)(2,1)} %param.26) | copy-start | bytes 589828
  6.5 4.2 %copy-start.1 = (bf16[128,768]{1,0:T(8,128)(2,1)S(1)}, bf16[128,768]{1,0:T(8,128)(2,1)}, u32[]{:S(2)}) copy-start(bf16[128,768]{1,0:T(8,128)(2,1)} %param.27) | copy-start | bytes 589828
  6.5 5.0 %copy-start = (bf16[1,384,256]{2,1,0:T(8,128)(2,1)S(1)}, bf16[1,384,256]{2,1,0:T(8,128)(2,1)}, u32[]{:S(2)}) copy-start(bf16[1,384,256]{2,1,0:T(8,128)(2,1)} %param.15) | copy-start | bytes 589828
  6.5 67.4 %all-gather.6.cloned.1.call-start = ((), (), s32[]{:S(2)}) async-start(), calls=%async_computation.11 | async-start | bytes 6684672 | tf_op jit(solution)/shard_map/all_gather | solution.py:53
  8.4 118.0 %all-gather.8.cloned.1.call-start = ((), (), s32[]{:S(2)}) async-start(), calls=%async_computation.12 | async-start | bytes 3342336 | tf_op jit(solution)/shard_map/all_gather | solution.py:84
  9.2 167.1 %all-gather.10.cloned.1.call-start = ((), (), s32[]{:S(2)}) async-start(), calls=%async_computation.13 | async-start | bytes 1114112 | tf_op jit(solution)/shard_map/all_gather | solution.py:53
  10.7 262.6 %all-gather.12.cloned.1.call-start = ((), (), s32[]{:S(2)}) async-start(), calls=%async_computation.14 | async-start | bytes 6684672 | tf_op jit(solution)/shard_map/all_gather | solution.py:53
  159.5 5.3 %copy-start.6 = (bf16[256]{0:T(256)(128)(2,1)S(1)}, bf16[256]{0:T(256)(128)(2,1)}, u32[]{:S(2)}) copy-start(bf16[256]{0:T(256)(128)(2,1)} %param.19) | copy-start | bytes 1540
  160.6 9.0 %all-to-all-start.2 = ((f32[8,1,768]{2,1,0:T(1,128)}), f32[8,1,768]{2,1,0:T(1,128)S(1)}, u32[]{:S(2)}, u32[]{:S(2)}) async-start(f32[8,1,768]{2,1,0:T(1,128)} %broadcast_in_dim.30), calls=%async_computation.2 | async-start | bytes 49152 | tf_op jit(solution)/shard_map/all_to_all | solution.py:12
  171.2 4.9 %copy-start.4 = (bf16[31,128]{1,0:T(8,128)(2,1)S(1)}, bf16[31,128]{1,0:T(8,128)(2,1)}, u32[]{:S(2)}) copy-start(bf16[31,128]{1,0:T(8,128)(2,1)} %param.22) | copy-start | bytes 23812
  171.2 25.0 %all-to-all-start.3 = ((bf16[8,384,256]{1,2,0:T(8,128)(2,1)}), bf16[8,384,256]{1,2,0:T(8,128)(2,1)S(1)}, u32[]{:S(2)}, u32[]{:S(2)}) async-start(bf16[8,384,256]{1,2,0:T(8,128)(2,1)} %broadcast_in_dim.31), calls=%async_computation.3 | async-start | bytes 3145728 | tf_op jit(solution)/shard_map/all_to_all | solution.py:12
  175.6 123.1 %all-gather.14.cloned.1.call-start = ((), (), s32[]{:S(2)}) async-start(), calls=%async_computation.15 | async-start | bytes 3342336 | tf_op jit(solution)/shard_map/all_gather | solution.py:84
  196.2 1.8 copy-start.5
  198.0 6.3 %copy-start.3 = (bf16[128,128]{1,0:T(8,128)(2,1)S(1)}, bf16[128,128]{1,0:T(8,128)(2,1)}, u32[]{:S(2)}) copy-start(bf16[128,128]{1,0:T(8,128)(2,1)} %param.24) | copy-start | bytes 98308
  198.6 15.9 %copy-start.7 = (bf16[128]{0:T(256)(128)(2,1)S(1)}, bf16[128]{0:T(256)(128)(2,1)}, u32[]{:S(2)}) copy-start(bf16[128]{0:T(256)(128)(2,1)} %param.23) | copy-start | bytes 772
  200.0 8.9 %all-to-all-start.4 = ((f32[8,1,768]{2,1,0:T(1,128)}), f32[8,1,768]{2,1,0:T(1,128)S(1)}, u32[]{:S(2)}, u32[]{:S(2)}) async-start(f32[8,1,768]{2,1,0:T(1,128)} %broadcast_in_dim.32), calls=%async_computation.4 | async-start | bytes 49152 | tf_op jit(solution)/shard_map/all_to_all | solution.py:12
  209.8 21.7 %all-to-all-start.5 = ((bf16[16,128,128]{1,2,0:T(8,128)(2,1)}), bf16[16,128,128]{1,2,0:T(8,128)(2,1)S(1)}, u32[]{:S(2)}, u32[]{:S(2)}) async-start(bf16[16,128,128]{1,2,0:T(8,128)(2,1)} %broadcast_in_dim.33), calls=%async_computation.5 | async-start | bytes 1048576 | tf_op jit(solution)/shard_map/all_to_all | solution.py:12
  257.3 5.3 %copy-start.8 = (bf16[256]{0:T(256)(128)(2,1)S(1)}, bf16[256]{0:T(256)(128)(2,1)}, u32[]{:S(2)}) copy-start(bf16[256]{0:T(256)(128)(2,1)} %param.25) | copy-start | bytes 1540
  258.4 9.0 %all-to-all-start.7 = ((f32[8,1,768]{2,1,0:T(1,128)}), f32[8,1,768]{2,1,0:T(1,128)S(1)}, u32[]{:S(2)}, u32[]{:S(2)}) async-start(f32[8,1,768]{2,1,0:T(1,128)} %broadcast_in_dim.34), calls=%async_computation.7 | async-start | bytes 49152 | tf_op jit(solution)/shard_map/all_to_all | solution.py:12
  269.1 24.8 %all-to-all-start.8 = ((bf16[8,384,256]{1,2,0:T(8,128)(2,1)}), bf16[8,384,256]{1,2,0:T(8,128)(2,1)S(1)}, u32[]{:S(2)}, u32[]{:S(2)}) async-start(bf16[8,384,256]{1,2,0:T(8,128)(2,1)} %broadcast_in_dim.35), calls=%async_computation.8 | async-start | bytes 3145728 | tf_op jit(solution)/shard_map/all_to_all | solution.py:12
  331.7 5.3 %copy-start.9 = (bf16[256]{0:T(256)(128)(2,1)S(1)}, bf16[256]{0:T(256)(128)(2,1)}, u32[]{:S(2)}) copy-start(bf16[256]{0:T(256)(128)(2,1)} %param.29) | copy-start | bytes 1540
  332.7 9.0 %all-to-all-start.10 = ((f32[8,1,768]{2,1,0:T(1,128)}), f32[8,1,768]{2,1,0:T(1,128)S(1)}, u32[]{:S(2)}, u32[]{:S(2)}) async-start(f32[8,1,768]{2,1,0:T(1,128)} %broadcast_in_dim.36), calls=%async_computation.10 | async-start | bytes 49152 | tf_op jit(solution)/shard_map/all_to_all | solution.py:12
Sparse Core Ops, SparseCore 0:
  9.5 64.3 all-gather.5
  76.0 50.3 all-gather.7
  128.6 41.5 all-gather.9
  172.1 67.7 all-gather.11
  241.9 50.3 all-gather.13
where the time goes:
time: 350 us; the launch traced here: 349 us
  waiting for transfers between devices  161 us (46%)
  blocking collectives  102 us (29%)
  starting transfers between devices  30.4 us (9%)
  matrix products  26.4 us (8%)
  between operations  13.4 us (4%)
  local copies, waits for them, and re-layouts  8.52 us (2%)
  other arithmetic  7.67 us (2%)
    all_to_all x7, waiting for transfers between devices, sent_to_all(): return lax.all_to_all(copies, axis, split_axis=0, concat_axis=0, tiled=True)  76.2 us
    all_to_all x3, blocking collectives, sent_and_summed(): lax.all_to_all(blocks, axis, split_axis=0, concat_axis=0, tiled=True)  75.6 us
    all_gather x2, waiting for transfers between devices, feed_forward(): full_down = lax.all_gather(w_down, 'fs', axis=1, tiled=True)  47.8 us
    all_gather x3, waiting for transfers between devices, sent_together(): out = lax.all_gather(both, axis, axis=dim, tiled=True)  35.9 us
    all_to_all x7, starting transfers between devices, sent_to_all(): return lax.all_to_all(copies, axis, split_axis=0, concat_axis=0, tiled=True)  30.2 us
    all_to_all x1, blocking collectives, sent_to_all(): return lax.all_to_all(copies, axis, split_axis=0, concat_axis=0, tiled=True)  26.1 us
    dot_general x2, matrix products, feed_forward(): jnp.dot(hidden, full_down, preferred_element_type=jnp.float32)  13.9 us
    dot_general x3, matrix products, fold_rows(): jnp.dot(gathered, shard_rows[0], preferred_element_type=jnp.float32)  11.2 us
  transfers between devices with their start and end apart: 12, of which 9 were waited for; matrix products, arithmetic and copies ran while one was open for 8% of the time, Pallas kernels for 0%

commit v1 on v0

v1 whole, which is shorter than its diff:
```python
import jax
import jax.numpy as jnp
from jax import lax
from jax.sharding import PartitionSpec as P

ALPHA = 2.0**0.25
EPSILON = 1e-05
F32 = jnp.float32
BF16 = jnp.bfloat16


def pull(value, axis, distance):
    if axis == "z":
        pairs = [(i, ((i // 4 - distance) % 4) * 4 + i % 4) for i in range(16)]
    elif axis == "y":
        pairs = [(i, (i // 4) * 4 + (i % 4 - distance) % 4) for i in range(16)]
    elif axis == "x":
        pairs = [(i, ((i // 2 - distance) % 4) * 2 + i % 2) for i in range(8)]
    else:
        pairs = [(i, i ^ 1) for i in range(8)]
    return lax.ppermute(value, "fs" if axis in "zy" else "tp", pairs)


def neighbours(value, axis):
    return pull(value, axis, 1), pull(value, axis, -1)


def opposite(after, before, axis):
    half = after.shape[0] // 2
    return pull(after[:half], axis, 1), pull(before[half:], axis, -1)


def in_ring(value, near, far):
    return jnp.concatenate([value, near[0], *far, near[1]], axis=0)


def matmul(left, right):
    return jnp.dot(left, right, preferred_element_type=F32)


def matmul_t(left, right):
    return lax.dot_general(left, right, (((1,), (1,)), ((), ())), preferred_element_type=F32)


def rolled(value, axis, shift):
    return lax.dynamic_slice_in_dim(
        jnp.concatenate([value, value], axis=axis), shift, value.shape[axis], axis
    )


def norm_rows(values, gain):
    center = jnp.mean(values, axis=-1, keepdims=True)
    off = values - center
    spread = jnp.mean(off * off, axis=-1, keepdims=True)
    return (off * lax.rsqrt(spread + EPSILON) * gain).astype(BF16)


SIDES = (0, 1, 3, 2)


def across(value):
    blocks = [value] + [pull(value, "x", d) for d in (2, 1, 3)]
    near = jnp.concatenate([blocks[0], blocks[2], blocks[3]], axis=0)
    return near, blocks[1], pull(near, "c", 1), pull(blocks[1], "c", 1)


def summed_rows(rows_other, rows_own):
    came = pull(rows_other.astype(BF16), "c", 1)
    pair = rows_own + came.astype(F32)
    count = pair.shape[0] // 4
    pieces = [pair[count * d : count * (d + 1)] for d in range(4)]
    total = pieces[0]
    for d in (2, 1, 3):
        total = total + pull(pieces[(-d) % 4].astype(BF16), "x", d).astype(F32)
    return total


def by_owner(value, x, core):
    split = value.reshape(4, 2, -1, value.shape[-1])
    out = []
    for c in (1 - core, core):
        part = lax.dynamic_index_in_dim(split, c, 1, keepdims=False)
        out.append(rolled(part, 0, x).reshape(-1, value.shape[-1]))
    return out


def in_order(blocks, x, core):
    flat = jnp.stack(
        [
            jnp.stack([jnp.where(core == 0, a, b), jnp.where(core == 0, b, a)])
            for a, b in blocks
        ]
    )
    return rolled(flat, 0, (4 - x) % 4).reshape(-1, flat.shape[-1])


def channel_stats(mixed):
    count = mixed.shape[-1]
    mean = jnp.sum(mixed, axis=-1) / count
    off = mixed - mean[:, None]
    square = jnp.sum(off * off, axis=-1)
    both = jnp.concatenate([mean, square]).reshape(1, 1, -1)
    both = jnp.broadcast_to(both, (8, 1, both.shape[-1]))
    both = lax.all_to_all(both, "tp", split_axis=0, concat_axis=0, tiled=True)
    mean, square = both[:, 0, : mean.size], both[:, 0, mean.size :]
    center = jnp.mean(mean, axis=0)
    off = mean - center
    spread = jnp.mean(square, axis=0) / count + jnp.mean(off * off, axis=0)
    return center[:, None], spread[:, None]


def body(
    tokens,
    first_gate,
    first_up,
    first_down,
    first_gain,
    glu_value,
    glu_gate,
    conv_taps,
    conv_gain,
    conv_proj,
    second_gain,
    last_gate,
    last_up,
    last_down,
    third_gain,
):
    tp = lax.axis_index("tp")
    fs = lax.axis_index("fs")
    x, core = tp // 2, tp % 2
    z, y = fs // 4, fs % 4
    current = tokens[0]

    early = lax.all_gather(
        jnp.concatenate([first_down.T, glu_value, glu_gate, conv_proj.T], axis=1),
        "fs",
        axis=0,
        tiled=True,
    )
    late = lax.all_gather(
        jnp.concatenate([last_gate, last_up, last_down.T], axis=1), "fs", axis=0, tiled=True
    )

    near_gate, near_up = neighbours(first_gate, "z"), neighbours(first_up, "y")
    far_gate, far_up = opposite(*near_gate, "z"), opposite(*near_up, "y")
    gate_part = in_ring(first_gate, near_gate, far_gate)
    up_part = in_ring(first_up, near_up, far_up)

    length = current.shape[0]
    gains = jnp.stack([first_gain, second_gain, third_gain])
    rows = jnp.concatenate([current, jnp.pad(gains, ((0, 5), (0, 0)))], axis=0)
    rows, _, _ = lax.optimization_barrier((rows, gate_part, up_part))
    blocks = [rows] + [pull(rows, "x", d) for d in (1, 2, 3)]
    blocks = [jnp.concatenate([b, pull(b, "c", 1)], axis=1) for b in blocks]
    turned = [rolled(b[:length], 1, ((y + 2 * core) % 4) * 128) for b in blocks]
    turned = rolled(jnp.concatenate(turned, axis=1), 1, ((z - x) % 4) * 512)
    some = [
        jnp.concatenate(
            [lax.dynamic_slice_in_dim(b, 48 * tp, 48, 0), b[length : length + 8]], axis=0
        )
        for b in blocks
    ]
    some = [rolled(b, 1, core * 256) for b in some]
    some = rolled(jnp.concatenate(some, axis=1), 1, ((4 - x) % 4) * 512)
    own_rows, gains = some[:48].astype(F32), some[48:51].astype(F32)

    near_gate, near_up = neighbours(gate_part, "y"), neighbours(up_part, "z")
    near_gate, near_up, turned = lax.optimization_barrier((near_gate, near_up, turned))
    far_gate, far_up = opposite(*near_gate, "y"), opposite(*near_up, "z")
    gate_of = [
        jnp.concatenate([turned[:, 512 * k + 128 * d :][:, :128] for k in range(4)], axis=1)
        for d in range(4)
    ]
    up_of = [turned[:, 512 * d : 512 * (d + 1)] for d in range(4)]

    def split_sum(left, own, near, far):
        total = matmul(left[0], own)
        total = total + matmul(left[1], near[0])
        total = total + matmul(left[3], near[1])
        total = total + matmul(left[2][:, :256], far[0])
        return total + matmul(left[2][:, 256:], far[1])

    gate = split_sum(gate_of, gate_part, near_gate, far_gate)
    up = split_sum(up_of, up_part, near_up, far_up)
    hidden = (jax.nn.silu(gate) * up).astype(BF16)

    def down(rows_other, rows_own, weight):
        return summed_rows(matmul_t(rows_other, weight), matmul_t(rows_own, weight))

    branch = down(*by_owner(hidden, x, core), early[:, :768])
    first = norm_rows(ALPHA * own_rows + 0.5 * branch, gains[0])

    def every_row(rows):
        near, far, near_other, far_other = across(rows)
        return jnp.concatenate([near, far, near_other, far_other], axis=0)

    def by_distance(values):
        count = values.shape[0] // 8
        at = [values[count * k : count * (k + 1)] for k in range(8)]
        own = [at[SIDES.index(d)] for d in range(4)]
        other = [at[4 + SIDES.index(d)] for d in range(4)]
        return own, other

    def gated_linear(rows):
        both = matmul(rows, early[:, 768:1024])
        return both[:, :128] * jax.nn.sigmoid(both[:, 128:])

    gated = in_order(list(zip(*by_distance(gated_linear(every_row(first))))), x, core)
    reach = (conv_taps.shape[0] - 1) // 2
    padded = jnp.pad(gated, ((reach, reach), (0, 0)))
    taps = conv_taps.astype(F32)
    mixed = jnp.zeros_like(gated)
    for k in range(conv_taps.shape[0]):
        mixed = mixed + taps[k] * padded[k : k + length]
    center, spread = channel_stats(mixed)
    normed = (mixed - center) * lax.rsqrt(spread + EPSILON) * conv_gain.astype(F32)
    act = jax.nn.silu(normed).astype(BF16)
    branch = down(*by_owner(act, x, core), early[:, 1024:])
    second = norm_rows(ALPHA * first.astype(F32) + branch, gains[1])

    def gated_hidden(rows):
        return (
            jax.nn.silu(matmul(rows, late[:, :768])) * matmul(rows, late[:, 768:1536])
        ).astype(BF16)

    own, other = by_distance(gated_hidden(every_row(second)))
    branch = down(
        jnp.concatenate(other, axis=0), jnp.concatenate(own, axis=0), late[:, 1536:]
    )
    out = norm_rows(ALPHA * second.astype(F32) + 0.5 * branch, gains[2])
    out = out.reshape(-1, 8, 256).transpose(1, 0, 2)
    out = lax.all_to_all(out, "tp", split_axis=0, concat_axis=0, tiled=True)
    return out.reshape(1, -1, 256)


def solution(mesh):
    return jax.shard_map(
        body,
        mesh=mesh,
        in_specs=(
            P("fs", None, "tp"),
            P("fs", "tp"),
            P("fs", "tp"),
            P("tp", "fs"),
            P("tp"),
            P("fs", "tp"),
            P("fs", "tp"),
            P(None, "tp"),
            P("tp"),
            P("tp", "fs"),
            P("tp"),
            P("fs", "tp"),
            P("fs", "tp"),
            P("tp", "fs"),
            P("tp"),
        ),
        out_specs=P("fs", None, "tp"),
        check_vma=False,
    )
```

time: 350 us -> 227 us (0.65)
  blocking collectives: 102 us -> 8.74 us
  waiting for transfers between devices: 161 us -> 110 us
  starting transfers between devices: 30.4 us -> 57.5 us
  matrix products: 26.4 us -> 20.2 us
    ppermute x0 -> x45, waiting for transfers between devices: none -> 105 us  [pull(): return lax.ppermute(value, 'fs' if axis in 'zy' else 'tp', pairs)]
    all_to_all x4 -> x1, blocking collectives: 102 us -> 8.74 us  [body(): out = lax.all_to_all(out, 'tp', split_axis=0, concat_axis=0, tiled=True)]
    all_gather x5 -> x2, waiting for transfers between devices: 83.7 us -> 0.04 us  [the longest x1 0.02 us: body(): lax.all_gather(jnp.concatenate([last_gate, last_up, last_down.T], axis=1)...]
    all_to_all x7 -> x1, waiting for transfers between devices: 76.2 us -> 4.75 us  [channel_stats(): both = lax.all_to_all(both, 'tp', split_axis=0, concat_axis=0, tiled=True)]
    ppermute x0 -> x45, starting transfers between devices: none -> 53.9 us  [pull(): return lax.ppermute(value, 'fs' if axis in 'zy' else 'tp', pairs)]
    all_to_all x7 -> x1, starting transfers between devices: 30.2 us -> 3.61 us  [channel_stats(): both = lax.all_to_all(both, 'tp', split_axis=0, concat_axis=0, tiled=True)]
    dot_general x7 -> x19, matrix products: 26.4 us -> 20.2 us  [the longest x13 11.9 us: matmul(): return jnp.dot(left, right, preferred_element_type=F32)]
    broadcast_in_dim x8 -> x1, local copies, waits for them, and re-layouts: 6.14 us -> 0.63 us  [channel_stats(): both = jnp.broadcast_to(both, (8, 1, both.shape[-1]))]
  transfers between devices with their start and end apart: 12 -> 48, of which waited for: 9 -> 33; matrix products, arithmetic and copies ran while one was open for 8% -> 10% of each run, Pallas kernels for 0% -> 0%
where the time goes in v1:
time: 227 us; the launch traced here: 226 us
  waiting for transfers between devices  110 us (48%)
  starting transfers between devices  57.5 us (25%)
  matrix products  20.2 us (9%)
  between operations  14.6 us (6%)
  blocking collectives  8.74 us (4%)
  other arithmetic  7.85 us (3%)
  local copies, waits for them, and re-layouts  7 us (3%)
    ppermute x45, waiting for transfers between devices, pull(): return lax.ppermute(value, 'fs' if axis in 'zy' else 'tp', pairs)  105 us
    ppermute x45, starting transfers between devices, pull(): return lax.ppermute(value, 'fs' if axis in 'zy' else 'tp', pairs)  53.9 us
    dot_general x13, matrix products, matmul(): return jnp.dot(left, right, preferred_element_type=F32)  11.9 us
    all_to_all x1, blocking collectives, body(): out = lax.all_to_all(out, 'tp', split_axis=0, concat_axis=0, tiled=True)  8.74 us
    dot_general x6, matrix products, matmul_t(): lax.dot_general(left, right, (((1,), (1,)), ((), ())), preferred_element_...  8.28 us
    unnamed x54, local copies, waits for them, and re-layouts  5.06 us
    all_to_all x1, waiting for transfers between devices, channel_stats(): both = lax.all_to_all(both, 'tp', split_axis=0, concat_axis=0, tiled=True)  4.75 us
  transfers between devices with their start and end apart: 48, of which 33 were waited for; matrix products, arithmetic and copies ran while one was open for 10% of the time, Pallas kernels for 0%

profile of v1, /device:TPU:1, one launch (start us, length us, event | category | flops | bytes accessed | tf_op | source)
XLA Modules:
  0.0 226.1 jit_solution(17102772664366023810)
XLA Ops:
  8.3 1.7 pad_maximum_fusion.3
  10.1 4.6 %collective-permute-start = (bf16[128,768]{1,0:T(8,128)(2,1)}, bf16[128,768]{1,0:T(8,128)(2,1)S(1)}, u32[]{:S(2)}, u32[]{:S(2)}) collective-permute-start(bf16[128,768]{1,0:T(8,128)(2,1)} %param.16), channel_id=1, source_target_pairs={{0,96},{8,104},{16,112},{24,120},{32,0},{40,8},{48,16},{56,24},{64... | collective-permute-start | bytes 589832 | tf_op jit(solution)/shard_map/ppermute | solution.py:21
  14.7 2.7 %collective-permute-start.4 = (bf16[128,768]{1,0:T(8,128)(2,1)}, bf16[128,768]{1,0:T(8,128)(2,1)S(1)}, u32[]{:S(2)}, u32[]{:S(2)}) collective-permute-start(bf16[128,768]{1,0:T(8,128)(2,1)} %param.17), channel_id=1, source_target_pairs={{0,24},{8,0},{16,8},{24,16},{32,56},{40,32},{48,40},{56,48},{64,88... | collective-permute-start | bytes 589832 | tf_op jit(solution)/shard_map/ppermute | solution.py:21
  20.9 2.7 %collective-permute-start.1 = (bf16[64,768]{1,0:T(8,128)(2,1)S(1)}, bf16[64,768]{1,0:T(8,128)(2,1)S(1)}, u32[]{:S(2)}, u32[]{:S(2)}) collective-permute-start(bf16[64,768]{1,0:T(8,128)(2,1)S(1)} %slice.605), channel_id=1, source_target_pairs={{0,96},{8,104},{16,112},{24,120},{32,0},{40,8},{48,16},{56,24},{64... | collective-permute-start | bytes 294920 | tf_op jit(solution)/shard_map/ppermute | solution.py:21
  23.8 2.7 %collective-permute-start.5 = (bf16[64,768]{1,0:T(8,128)(2,1)S(1)}, bf16[64,768]{1,0:T(8,128)(2,1)S(1)}, u32[]{:S(2)}, u32[]{:S(2)}) collective-permute-start(bf16[64,768]{1,0:T(8,128)(2,1)S(1)} %slice.607), channel_id=1, source_target_pairs={{0,24},{8,0},{16,8},{24,16},{32,56},{40,32},{48,40},{56,48},{64,88... | collective-permute-start | bytes 294920 | tf_op jit(solution)/shard_map/ppermute | solution.py:21
  26.9 3.5 %collective-permute-done.3 = bf16[64,768]{1,0:T(8,128)(2,1)S(1)} collective-permute-done((bf16[64,768]{1,0:T(8,128)(2,1)S(1)}, bf16[64,768]{1,0:T(8,128)(2,1)S(1)}, u32[]{:S(2)}, u32[]{:S(2)}) %collective-permute-start.3) | collective-permute-done | bytes 98336 | tf_op jit(solution)/shard_map/ppermute | solution.py:21
  30.5 2.0 collective-permute-done.7
  32.5 2.4 %collective-permute-start.8 = (bf16[392,256]{1,0:T(8,128)(2,1)S(1)}, bf16[392,256]{1,0:T(8,128)(2,1)S(1)}, u32[]{:S(2)}, u32[]{:S(2)}) collective-permute-start(bf16[392,256]{1,0:T(8,128)(2,1)S(1)} %pad_maximum_fusion.4), channel_id=1, source_target_pairs={{0,1},{1,0},{2,3},{3,2},{4,5},{5,4},{6,7},{7,6},{8,9},{9,8},{10,11... | collective-permute-start | bytes 602120 | tf_op jit(solution)/shard_map/ppermute | solution.py:21
  34.9 2.6 %collective-permute-start.9 = (bf16[392,256]{1,0:T(8,128)(2,1)S(1)}, bf16[392,256]{1,0:T(8,128)(2,1)S(1)}, u32[]{:S(2)}, u32[]{:S(2)}) collective-permute-start(bf16[392,256]{1,0:T(8,128)(2,1)S(1)} %pad_maximum_fusion.4), channel_id=1, source_target_pairs={{0,6},{1,7},{2,0},{3,1},{4,2},{5,3},{6,4},{7,5},{8,14},{9,15},{10,... | collective-permute-start | bytes 602120 | tf_op jit(solution)/shard_map/ppermute | solution.py:21
  40.4 5.4 %collective-permute-done.9 = bf16[392,256]{1,0:T(8,128)(2,1)S(1)} collective-permute-done((bf16[392,256]{1,0:T(8,128)(2,1)S(1)}, bf16[392,256]{1,0:T(8,128)(2,1)S(1)}, u32[]{:S(2)}, u32[]{:S(2)}) %collective-permute-start.9) | collective-permute-done | bytes 200736 | tf_op jit(solution)/shard_map/ppermute | solution.py:21
  45.8 3.7 %collective-permute-start.17 = (bf16[512,768]{1,0:T(8,128)(2,1)S(1)}, bf16[512,768]{1,0:T(8,128)(2,1)S(1)}, u32[]{:S(2)}, u32[]{:S(2)}) collective-permute-start(bf16[512,768]{1,0:T(8,128)(2,1)S(1)} %constant_dynamic-update-slice_fusion.5), channel_id=1, source_target_pairs={{0,96},{8,104},{16,112},{24,120},{32,0},{40,8},{48,16},{56,24},{64... | collective-permute-start | bytes 2359304 | tf_op jit(solution)/shard_map/ppermute | solution.py:21
  49.5 1.5 collective-permute-start.10
  55.3 7.8 %collective-permute-done.15 = bf16[512,768]{1,0:T(8,128)(2,1)S(1)} collective-permute-done((bf16[512,768]{1,0:T(8,128)(2,1)S(1)}, bf16[512,768]{1,0:T(8,128)(2,1)S(1)}, u32[]{:S(2)}, u32[]{:S(2)}) %collective-permute-start.15) | collective-permute-done | bytes 786464 | tf_op jit(solution)/shard_map/ppermute | solution.py:21
  63.1 2.0 collective-permute-done.16
  65.2 12.1 %collective-permute-done.17 = bf16[512,768]{1,0:T(8,128)(2,1)S(1)} collective-permute-done((bf16[512,768]{1,0:T(8,128)(2,1)S(1)}, bf16[512,768]{1,0:T(8,128)(2,1)S(1)}, u32[]{:S(2)}, u32[]{:S(2)}) %collective-permute-start.17) | collective-permute-done | bytes 786464 | tf_op jit(solution)/shard_map/ppermute | solution.py:21
  77.3 8.3 %collective-permute-done.18 = bf16[512,768]{1,0:T(8,128)(2,1)S(1)} collective-permute-done((bf16[512,768]{1,0:T(8,128)(2,1)S(1)}, bf16[512,768]{1,0:T(8,128)(2,1)S(1)}, u32[]{:S(2)}, u32[]{:S(2)}) %collective-permute-start.18) | collective-permute-done | bytes 786464 | tf_op jit(solution)/shard_map/ppermute | solution.py:21
  85.6 1.7 collective-permute-start.21
  91.6 5.3 %collective-permute-done.19 = bf16[256,768]{1,0:T(8,128)(2,1)S(1)} collective-permute-done((bf16[256,768]{1,0:T(8,128)(2,1)S(1)}, bf16[256,768]{1,0:T(8,128)(2,1)S(1)}, u32[]{:S(2)}, u32[]{:S(2)}) %collective-permute-start.19) | collective-permute-done | bytes 393248 | tf_op jit(solution)/shard_map/ppermute | solution.py:21
  100.9 3.1 %fusion.12 = bf16[192,2048]{1,0:T(8,128)(2,1)S(1)} fusion(bf16[192,768]{1,0:T(8,128)(2,1)S(1)} %bitcast.164, bf16[2048,1152]{0,1:T(8,128)(2,1)} %all-gather.3.cloned.1.call-done), kind=kOutput, calls=%fused_computation.12 | convolution fusion | flops 604372992 | bytes 4227072 | tf_op jit(solution)/shard_map/dot_general | solution.py:42
  104.0 2.5 %collective-permute-start.23 = (bf16[192,2048]{1,0:T(8,128)(2,1)S(1)}, bf16[192,2048]{1,0:T(8,128)(2,1)S(1)}, u32[]{:S(2)}, u32[]{:S(2)}) collective-permute-start(bf16[192,2048]{1,0:T(8,128)(2,1)S(1)} %fusion.12), channel_id=1, source_target_pairs={{0,1},{1,0},{2,3},{3,2},{4,5},{5,4},{6,7},{7,6},{8,9},{9,8},{10,11... | collective-permute-start | bytes 2359304 | tf_op jit(solution)/shard_map/ppermute | solution.py:21
  106.7 1.7 collective-permute-done.23
  109.3 1.9 collective-permute-start.24
  112.7 4.3 %collective-permute-done.24 = bf16[48,2048]{1,0:T(8,128)(2,1)S(1)} collective-permute-done((bf16[48,2048]{1,0:T(8,128)(2,1)S(1)}, bf16[48,2048]{1,0:T(8,128)(2,1)S(1)}, u32[]{:S(2)}, u32[]{:S(2)}) %collective-permute-start.24) | collective-permute-done | bytes 196640 | tf_op jit(solution)/shard_map/ppermute | solution.py:21
  117.0 4.0 %collective-permute-done.25 = bf16[48,2048]{1,0:T(8,128)(2,1)S(1)} collective-permute-done((bf16[48,2048]{1,0:T(8,128)(2,1)S(1)}, bf16[48,2048]{1,0:T(8,128)(2,1)S(1)}, u32[]{:S(2)}, u32[]{:S(2)}) %collective-permute-start.25) | collective-permute-done | bytes 196640 | tf_op jit(solution)/shard_map/ppermute | solution.py:21
  122.4 2.3 %collective-permute-start.27 = (bf16[48,2048]{1,0:T(8,128)(2,1)S(1)}, bf16[48,2048]{1,0:T(8,128)(2,1)S(1)}, u32[]{:S(2)}, u32[]{:S(2)}) collective-permute-start(bf16[48,2048]{1,0:T(8,128)(2,1)S(1)} %get-tuple-element.28), channel_id=1, source_target_pairs={{0,6},{1,7},{2,0},{3,1},{4,2},{5,3},{6,4},{7,5},{8,14},{9,15},{10,... | collective-permute-start | bytes 589832 | tf_op jit(solution)/shard_map/ppermute | solution.py:21
  126.0 2.4 %collective-permute-done.27 = bf16[48,2048]{1,0:T(8,128)(2,1)S(1)} collective-permute-done((bf16[48,2048]{1,0:T(8,128)(2,1)S(1)}, bf16[48,2048]{1,0:T(8,128)(2,1)S(1)}, u32[]{:S(2)}, u32[]{:S(2)}) %collective-permute-start.27) | collective-permute-done | bytes 196640 | tf_op jit(solution)/shard_map/ppermute | solution.py:21
  128.4 7.5 %collective-permute-done.28 = bf16[48,2048]{1,0:T(8,128)(2,1)S(1)} collective-permute-done((bf16[48,2048]{1,0:T(8,128)(2,1)S(1)}, bf16[48,2048]{1,0:T(8,128)(2,1)S(1)}, u32[]{:S(2)}, u32[]{:S(2)}) %collective-permute-start.28) | collective-permute-done | bytes 196640 | tf_op jit(solution)/shard_map/ppermute | solution.py:21
  136.0 1.6 collective-permute-start.30
  137.7 1.5 collective-permute-done.30
  142.0 3.6 %all-to-all-start = ((f32[8,1,768]{2,1,0:T(1,128)}), f32[8,1,768]{2,1,0:T(1,128)S(1)}, u32[]{:S(2)}, u32[]{:S(2)}) async-start(f32[8,1,768]{2,1,0:T(1,128)} %broadcast_in_dim.2), calls=%async_computation | async-start | bytes 49152 | tf_op jit(solution)/shard_map/all_to_all | solution.py:104
  145.6 4.8 %all-to-all-done = f32[8,1,768]{2,1,0:T(1,128)S(1)} async-done(((f32[8,1,768]{2,1,0:T(1,128)}), f32[8,1,768]{2,1,0:T(1,128)S(1)}, u32[]{:S(2)}, u32[]{:S(2)}) %all-to-all-start) | async-done | bytes 24608 | tf_op jit(solution)/shard_map/all_to_all | solution.py:104
  150.7 1.4 convolution_convert_fusion
  152.9 1.9 collective-permute-done.32
  157.2 1.8 collective-permute-start.34
  159.1 4.8 %collective-permute-done.33 = bf16[48,2048]{1,0:T(8,128)(2,1)S(1)} collective-permute-done((bf16[48,2048]{1,0:T(8,128)(2,1)S(1)}, bf16[48,2048]{1,0:T(8,128)(2,1)S(1)}, u32[]{:S(2)}, u32[]{:S(2)}) %collective-permute-start.33) | collective-permute-done | bytes 196640 | tf_op jit(solution)/shard_map/ppermute | solution.py:21
  163.9 2.8 %collective-permute-done.34 = bf16[48,2048]{1,0:T(8,128)(2,1)S(1)} collective-permute-done((bf16[48,2048]{1,0:T(8,128)(2,1)S(1)}, bf16[48,2048]{1,0:T(8,128)(2,1)S(1)}, u32[]{:S(2)}, u32[]{:S(2)}) %collective-permute-start.34) | collective-permute-done | bytes 196640 | tf_op jit(solution)/shard_map/ppermute | solution.py:21
  166.8 2.1 collective-permute-done.35
  172.0 3.5 %collective-permute-done.36 = bf16[48,2048]{1,0:T(8,128)(2,1)S(1)} collective-permute-done((bf16[48,2048]{1,0:T(8,128)(2,1)S(1)}, bf16[48,2048]{1,0:T(8,128)(2,1)S(1)}, u32[]{:S(2)}, u32[]{:S(2)}) %collective-permute-start.36) | collective-permute-done | bytes 196640 | tf_op jit(solution)/shard_map/ppermute | solution.py:21
  175.5 3.3 %collective-permute-done.37 = bf16[48,2048]{1,0:T(8,128)(2,1)S(1)} collective-permute-done((bf16[48,2048]{1,0:T(8,128)(2,1)S(1)}, bf16[48,2048]{1,0:T(8,128)(2,1)S(1)}, u32[]{:S(2)}, u32[]{:S(2)}) %collective-permute-start.37) | collective-permute-done | bytes 196640 | tf_op jit(solution)/shard_map/ppermute | solution.py:21
  178.8 4.6 %collective-permute-start.39 = (bf16[144,2048]{1,0:T(8,128)(2,1)S(1)}, bf16[144,2048]{1,0:T(8,128)(2,1)S(1)}, u32[]{:S(2)}, u32[]{:S(2)}) collective-permute-start(bf16[144,2048]{1,0:T(8,128)(2,1)S(1)} %pad_maximum_fusion.1), channel_id=1, source_target_pairs={{0,1},{1,0},{2,3},{3,2},{4,5},{5,4},{6,7},{7,6},{8,9},{9,8},{10,11... | collective-permute-start | bytes 1769480 | tf_op jit(solution)/shard_map/ppermute | solution.py:21
  183.6 1.5 collective-permute-done.39
  185.4 3.5 %fusion.2 = f32[384,768]{1,0:T(8,128)S(1)} fusion(bf16[384,2048]{1,0:T(8,128)(2,1)S(1)} %constant_dynamic-update-slice_fusion.48, bf16[2048,2304]{0,1:T(8,128)(2,1)} %all-gather.5.cloned.1.call-done), kind=kOutput, calls=%fused_computation.2 | convolution fusion | flops 1207959552 | bytes 5898240 | tf_op jit(solution)/shard_map/dot_general | solution.py:38
  188.9 3.5 %multiply_convert_fusion = bf16[384,768]{1,0:T(8,128)(2,1)S(1)} fusion(f32[384,768]{1,0:T(8,128)S(1)} %fusion.2, bf16[384,2048]{1,0:T(8,128)(2,1)S(1)} %constant_dynamic-update-slice_fusion.48, bf16[2048,2304]{0,1:T(8,128)(2,1)} %all-gather.5.cloned.1.call-done), kind=kOutput, calls=%fused_computation.26 | convolution fusion | flops 1209729024 | bytes 6488064 | tf_op jit(solution)/shard_map/dot_general | solution.py:38
  193.8 1.9 collective-permute-done.41
  196.7 1.5 collective-permute-start.44
  198.2 6.1 %collective-permute-done.42 = bf16[48,2048]{1,0:T(8,128)(2,1)S(1)} collective-permute-done((bf16[48,2048]{1,0:T(8,128)(2,1)S(1)}, bf16[48,2048]{1,0:T(8,128)(2,1)S(1)}, u32[]{:S(2)}, u32[]{:S(2)}) %collective-permute-start.42) | collective-permute-done | bytes 196640 | tf_op jit(solution)/shard_map/ppermute | solution.py:21
  205.4 3.8 %collective-permute-done.44 = bf16[48,2048]{1,0:T(8,128)(2,1)S(1)} collective-permute-done((bf16[48,2048]{1,0:T(8,128)(2,1)S(1)}, bf16[48,2048]{1,0:T(8,128)(2,1)S(1)}, u32[]{:S(2)}, u32[]{:S(2)}) %collective-permute-start.44) | collective-permute-done | bytes 196640 | tf_op jit(solution)/shard_map/ppermute | solution.py:21
  209.8 8.7 %all_to_all.10 = bf16[8,48,256]{2,1,0:T(8,128)(2,1)S(1)} all-to-all(bf16[8,48,256]{2,1,0:T(8,128)(2,1)S(1)} %bitcast.159), channel_id=1, replica_groups=mesh['fs'=16,'tp'=8] {'tp'}, dimensions={0} | all-to-all | bytes 393216 | tf_op jit(solution)/shard_map/all_to_all | solution.py:233
  (229 shorter events, 40.9 us)
Async XLA Ops:
  6.5 94.4 %all-gather.3.cloned.1.call-start = ((), (), s32[]{:S(2)}) async-start(), calls=%async_computation.2 | async-start | bytes 5013504 | tf_op jit(solution)/shard_map/all_gather | solution.py:135
  10.0 175.3 %all-gather.5.cloned.1.call-start = ((), (), s32[]{:S(2)}) async-start(), calls=%async_computation.3 | async-start | bytes 10027008 | tf_op jit(solution)/shard_map/all_gather | solution.py:141
  10.1 10.8 %collective-permute-start = (bf16[128,768]{1,0:T(8,128)(2,1)}, bf16[128,768]{1,0:T(8,128)(2,1)S(1)}, u32[]{:S(2)}, u32[]{:S(2)}) collective-permute-start(bf16[128,768]{1,0:T(8,128)(2,1)} %param.16), channel_id=1, source_target_pairs={{0,96},{8,104},{16,112},{24,120},{32,0},{40,8},{48,16},{56,24},{64... | collective-permute-start | bytes 589832 | tf_op jit(solution)/shard_map/ppermute | solution.py:21
  14.7 8.9 %collective-permute-start.2 = (bf16[128,768]{1,0:T(8,128)(2,1)}, bf16[128,768]{1,0:T(8,128)(2,1)S(1)}, u32[]{:S(2)}, u32[]{:S(2)}) collective-permute-start(bf16[128,768]{1,0:T(8,128)(2,1)} %param.16), channel_id=1, source_target_pairs={{0,32},{8,40},{16,48},{24,56},{32,64},{40,72},{48,80},{56,88},{64,... | collective-permute-start | bytes 589832 | tf_op jit(solution)/shard_map/ppermute | solution.py:21
  14.7 9.0 %collective-permute-start.4 = (bf16[128,768]{1,0:T(8,128)(2,1)}, bf16[128,768]{1,0:T(8,128)(2,1)S(1)}, u32[]{:S(2)}, u32[]{:S(2)}) collective-permute-start(bf16[128,768]{1,0:T(8,128)(2,1)} %param.17), channel_id=1, source_target_pairs={{0,24},{8,0},{16,8},{24,16},{32,56},{40,32},{48,40},{56,48},{64,88... | collective-permute-start | bytes 589832 | tf_op jit(solution)/shard_map/ppermute | solution.py:21
  17.5 9.0 %collective-permute-start.6 = (bf16[128,768]{1,0:T(8,128)(2,1)}, bf16[128,768]{1,0:T(8,128)(2,1)S(1)}, u32[]{:S(2)}, u32[]{:S(2)}) collective-permute-start(bf16[128,768]{1,0:T(8,128)(2,1)} %param.17), channel_id=1, source_target_pairs={{0,8},{8,16},{16,24},{24,0},{32,40},{40,48},{48,56},{56,32},{64,72... | collective-permute-start | bytes 589832 | tf_op jit(solution)/shard_map/ppermute | solution.py:21
  20.9 6.0 %collective-permute-start.1 = (bf16[64,768]{1,0:T(8,128)(2,1)S(1)}, bf16[64,768]{1,0:T(8,128)(2,1)S(1)}, u32[]{:S(2)}, u32[]{:S(2)}) collective-permute-start(bf16[64,768]{1,0:T(8,128)(2,1)S(1)} %slice.605), channel_id=1, source_target_pairs={{0,96},{8,104},{16,112},{24,120},{32,0},{40,8},{48,16},{56,24},{64... | collective-permute-start | bytes 294920 | tf_op jit(solution)/shard_map/ppermute | solution.py:21
  23.7 6.7 %collective-permute-start.3 = (bf16[64,768]{1,0:T(8,128)(2,1)S(1)}, bf16[64,768]{1,0:T(8,128)(2,1)S(1)}, u32[]{:S(2)}, u32[]{:S(2)}) collective-permute-start(bf16[64,768]{1,0:T(8,128)(2,1)S(1)} %slice.606), channel_id=1, source_target_pairs={{0,32},{8,40},{16,48},{24,56},{32,64},{40,72},{48,80},{56,88},{64,... | collective-permute-start | bytes 294920 | tf_op jit(solution)/shard_map/ppermute | solution.py:21
  23.8 6.7 %collective-permute-start.5 = (bf16[64,768]{1,0:T(8,128)(2,1)S(1)}, bf16[64,768]{1,0:T(8,128)(2,1)S(1)}, u32[]{:S(2)}, u32[]{:S(2)}) collective-permute-start(bf16[64,768]{1,0:T(8,128)(2,1)S(1)} %slice.607), channel_id=1, source_target_pairs={{0,24},{8,0},{16,8},{24,16},{32,56},{40,32},{48,40},{56,48},{64,88... | collective-permute-start | bytes 294920 | tf_op jit(solution)/shard_map/ppermute | solution.py:21
  26.5 6.0 %collective-permute-start.7 = (bf16[64,768]{1,0:T(8,128)(2,1)S(1)}, bf16[64,768]{1,0:T(8,128)(2,1)S(1)}, u32[]{:S(2)}, u32[]{:S(2)}) collective-permute-start(bf16[64,768]{1,0:T(8,128)(2,1)S(1)} %slice.608), channel_id=1, source_target_pairs={{0,8},{8,16},{16,24},{24,0},{32,40},{40,48},{48,56},{56,32},{64,72... | collective-permute-start | bytes 294920 | tf_op jit(solution)/shard_map/ppermute | solution.py:21
  32.5 7.1 %collective-permute-start.8 = (bf16[392,256]{1,0:T(8,128)(2,1)S(1)}, bf16[392,256]{1,0:T(8,128)(2,1)S(1)}, u32[]{:S(2)}, u32[]{:S(2)}) collective-permute-start(bf16[392,256]{1,0:T(8,128)(2,1)S(1)} %pad_maximum_fusion.4), channel_id=1, source_target_pairs={{0,1},{1,0},{2,3},{3,2},{4,5},{5,4},{6,7},{7,6},{8,9},{9,8},{10,11... | collective-permute-start | bytes 602120 | tf_op jit(solution)/shard_map/ppermute | solution.py:21
  34.9 10.9 %collective-permute-start.9 = (bf16[392,256]{1,0:T(8,128)(2,1)S(1)}, bf16[392,256]{1,0:T(8,128)(2,1)S(1)}, u32[]{:S(2)}, u32[]{:S(2)}) collective-permute-start(bf16[392,256]{1,0:T(8,128)(2,1)S(1)} %pad_maximum_fusion.4), channel_id=1, source_target_pairs={{0,6},{1,7},{2,0},{3,1},{4,2},{5,3},{6,4},{7,5},{8,14},{9,15},{10,... | collective-permute-start | bytes 602120 | tf_op jit(solution)/shard_map/ppermute | solution.py:21
  37.5 12.0 %collective-permute-start.11 = (bf16[392,256]{1,0:T(8,128)(2,1)S(1)}, bf16[392,256]{1,0:T(8,128)(2,1)S(1)}, u32[]{:S(2)}, u32[]{:S(2)}) collective-permute-start(bf16[392,256]{1,0:T(8,128)(2,1)S(1)} %pad_maximum_fusion.4), channel_id=1, source_target_pairs={{0,4},{1,5},{2,6},{3,7},{4,0},{5,1},{6,2},{7,3},{8,12},{9,13},{10,... | collective-permute-start | bytes 602120 | tf_op jit(solution)/shard_map/ppermute | solution.py:21
  38.0 13.1 %collective-permute-start.13 = (bf16[392,256]{1,0:T(8,128)(2,1)S(1)}, bf16[392,256]{1,0:T(8,128)(2,1)S(1)}, u32[]{:S(2)}, u32[]{:S(2)}) collective-permute-start(bf16[392,256]{1,0:T(8,128)(2,1)S(1)} %pad_maximum_fusion.4), channel_id=1, source_target_pairs={{0,2},{1,3},{2,4},{3,5},{4,6},{5,7},{6,0},{7,1},{8,10},{9,11},{10,... | collective-permute-start | bytes 602120 | tf_op jit(solution)/shard_map/ppermute | solution.py:21
  38.6 24.5 %collective-permute-start.15 = (bf16[512,768]{1,0:T(8,128)(2,1)S(1)}, bf16[512,768]{1,0:T(8,128)(2,1)S(1)}, u32[]{:S(2)}, u32[]{:S(2)}) collective-permute-start(bf16[512,768]{1,0:T(8,128)(2,1)S(1)} %constant_dynamic-update-slice_fusion), channel_id=1, source_target_pairs={{0,24},{8,0},{16,8},{24,16},{32,56},{40,32},{48,40},{56,48},{64,88... | collective-permute-start | bytes 2359304 | tf_op jit(solution)/shard_map/ppermute | solution.py:21
  39.6 25.5 %collective-permute-start.16 = (bf16[512,768]{1,0:T(8,128)(2,1)S(1)}, bf16[512,768]{1,0:T(8,128)(2,1)S(1)}, u32[]{:S(2)}, u32[]{:S(2)}) collective-permute-start(bf16[512,768]{1,0:T(8,128)(2,1)S(1)} %constant_dynamic-update-slice_fusion), channel_id=1, source_target_pairs={{0,8},{8,16},{16,24},{24,0},{32,40},{40,48},{48,56},{56,32},{64,72... | collective-permute-start | bytes 2359304 | tf_op jit(solution)/shard_map/ppermute | solution.py:21
  45.8 31.4 %collective-permute-start.17 = (bf16[512,768]{1,0:T(8,128)(2,1)S(1)}, bf16[512,768]{1,0:T(8,128)(2,1)S(1)}, u32[]{:S(2)}, u32[]{:S(2)}) collective-permute-start(bf16[512,768]{1,0:T(8,128)(2,1)S(1)} %constant_dynamic-update-slice_fusion.5), channel_id=1, source_target_pairs={{0,96},{8,104},{16,112},{24,120},{32,0},{40,8},{48,16},{56,24},{64... | collective-permute-start | bytes 2359304 | tf_op jit(solution)/shard_map/ppermute | solution.py:21
  49.5 2.6 %collective-permute-start.10 = (bf16[392,256]{1,0:T(8,128)(2,1)S(1)}, bf16[392,256]{1,0:T(8,128)(2,1)S(1)}, u32[]{:S(2)}, u32[]{:S(2)}) collective-permute-start(bf16[392,256]{1,0:T(8,128)(2,1)S(1)} %collective-permute-done.9), channel_id=1, source_target_pairs={{0,1},{1,0},{2,3},{3,2},{4,5},{5,4},{6,7},{7,6},{8,9},{9,8},{10,11... | collective-permute-start | bytes 602120 | tf_op jit(solution)/shard_map/ppermute | solution.py:21
  51.1 1.5 collective-permute-start.12
  52.1 1.4 collective-permute-start.14
  52.6 33.0 %collective-permute-start.18 = (bf16[512,768]{1,0:T(8,128)(2,1)S(1)}, bf16[512,768]{1,0:T(8,128)(2,1)S(1)}, u32[]{:S(2)}, u32[]{:S(2)}) collective-permute-start(bf16[512,768]{1,0:T(8,128)(2,1)S(1)} %constant_dynamic-update-slice_fusion.5), channel_id=1, source_target_pairs={{0,32},{8,40},{16,48},{24,56},{32,64},{40,72},{48,80},{56,88},{64,... | collective-permute-start | bytes 2359304 | tf_op jit(solution)/shard_map/ppermute | solution.py:21
  85.6 13.2 %collective-permute-start.21 = (bf16[256,768]{1,0:T(8,128)(2,1)S(1)}, bf16[256,768]{1,0:T(8,128)(2,1)S(1)}, u32[]{:S(2)}, u32[]{:S(2)}) collective-permute-start(bf16[256,768]{1,0:T(8,128)(2,1)S(1)} %slice.501), channel_id=1, source_target_pairs={{0,96},{8,104},{16,112},{24,120},{32,0},{40,8},{48,16},{56,24},{64... | collective-permute-start | bytes 1179656 | tf_op jit(solution)/shard_map/ppermute | solution.py:21
  87.3 11.8 %collective-permute-start.22 = (bf16[256,768]{1,0:T(8,128)(2,1)S(1)}, bf16[256,768]{1,0:T(8,128)(2,1)S(1)}, u32[]{:S(2)}, u32[]{:S(2)}) collective-permute-start(bf16[256,768]{1,0:T(8,128)(2,1)S(1)} %slice.503), channel_id=1, source_target_pairs={{0,32},{8,40},{16,48},{24,56},{32,64},{40,72},{48,80},{56,88},{64,... | collective-permute-start | bytes 1179656 | tf_op jit(solution)/shard_map/ppermute | solution.py:21
  87.5 9.4 %collective-permute-start.19 = (bf16[256,768]{1,0:T(8,128)(2,1)S(1)}, bf16[256,768]{1,0:T(8,128)(2,1)S(1)}, u32[]{:S(2)}, u32[]{:S(2)}) collective-permute-start(bf16[256,768]{1,0:T(8,128)(2,1)S(1)} %slice.493), channel_id=1, source_target_pairs={{0,24},{8,0},{16,8},{24,16},{32,56},{40,32},{48,40},{56,48},{64,88... | collective-permute-start | bytes 1179656 | tf_op jit(solution)/shard_map/ppermute | solution.py:21
  88.1 10.4 %collective-permute-start.20 = (bf16[256,768]{1,0:T(8,128)(2,1)S(1)}, bf16[256,768]{1,0:T(8,128)(2,1)S(1)}, u32[]{:S(2)}, u32[]{:S(2)}) collective-permute-start(bf16[256,768]{1,0:T(8,128)(2,1)S(1)} %slice.496), channel_id=1, source_target_pairs={{0,8},{8,16},{16,24},{24,0},{32,40},{40,48},{48,56},{56,32},{64,72... | collective-permute-start | bytes 1179656 | tf_op jit(solution)/shard_map/ppermute | solution.py:21
  104.0 4.4 %collective-permute-start.23 = (bf16[192,2048]{1,0:T(8,128)(2,1)S(1)}, bf16[192,2048]{1,0:T(8,128)(2,1)S(1)}, u32[]{:S(2)}, u32[]{:S(2)}) collective-permute-start(bf16[192,2048]{1,0:T(8,128)(2,1)S(1)} %fusion.12), channel_id=1, source_target_pairs={{0,1},{1,0},{2,3},{3,2},{4,5},{5,4},{6,7},{7,6},{8,9},{9,8},{10,11... | collective-permute-start | bytes 2359304 | tf_op jit(solution)/shard_map/ppermute | solution.py:21
  109.3 7.7 %collective-permute-start.24 = (bf16[48,2048]{1,0:T(8,128)(2,1)S(1)}, bf16[48,2048]{1,0:T(8,128)(2,1)S(1)}, u32[]{:S(2)}, u32[]{:S(2)}) collective-permute-start(bf16[48,2048]{1,0:T(8,128)(2,1)S(1)} %get-tuple-element.63), channel_id=1, source_target_pairs={{0,4},{1,5},{2,6},{3,7},{4,0},{5,1},{6,2},{7,3},{8,12},{9,13},{10,... | collective-permute-start | bytes 589832 | tf_op jit(solution)/shard_map/ppermute | solution.py:21
  111.2 9.7 %collective-permute-start.25 = (bf16[48,2048]{1,0:T(8,128)(2,1)S(1)}, bf16[48,2048]{1,0:T(8,128)(2,1)S(1)}, u32[]{:S(2)}, u32[]{:S(2)}) collective-permute-start(bf16[48,2048]{1,0:T(8,128)(2,1)S(1)} %get-tuple-element.65), channel_id=1, source_target_pairs={{0,6},{1,7},{2,0},{3,1},{4,2},{5,3},{6,4},{7,5},{8,14},{9,15},{10,... | collective-permute-start | bytes 589832 | tf_op jit(solution)/shard_map/ppermute | solution.py:21
  112.1 9.7 %collective-permute-start.26 = (bf16[48,2048]{1,0:T(8,128)(2,1)S(1)}, bf16[48,2048]{1,0:T(8,128)(2,1)S(1)}, u32[]{:S(2)}, u32[]{:S(2)}) collective-permute-start(bf16[48,2048]{1,0:T(8,128)(2,1)S(1)} %get-tuple-element.64), channel_id=1, source_target_pairs={{0,2},{1,3},{2,4},{3,5},{4,6},{5,7},{6,0},{7,1},{8,10},{9,11},{10,... | collective-permute-start | bytes 589832 | tf_op jit(solution)/shard_map/ppermute | solution.py:21
  122.4 6.0 %collective-permute-start.27 = (bf16[48,2048]{1,0:T(8,128)(2,1)S(1)}, bf16[48,2048]{1,0:T(8,128)(2,1)S(1)}, u32[]{:S(2)}, u32[]{:S(2)}) collective-permute-start(bf16[48,2048]{1,0:T(8,128)(2,1)S(1)} %get-tuple-element.28), channel_id=1, source_target_pairs={{0,6},{1,7},{2,0},{3,1},{4,2},{5,3},{6,4},{7,5},{8,14},{9,15},{10,... | collective-permute-start | bytes 589832 | tf_op jit(solution)/shard_map/ppermute | solution.py:21
  124.7 11.2 %collective-permute-start.28 = (bf16[48,2048]{1,0:T(8,128)(2,1)S(1)}, bf16[48,2048]{1,0:T(8,128)(2,1)S(1)}, u32[]{:S(2)}, u32[]{:S(2)}) collective-permute-start(bf16[48,2048]{1,0:T(8,128)(2,1)S(1)} %get-tuple-element.28), channel_id=1, source_target_pairs={{0,2},{1,3},{2,4},{3,5},{4,6},{5,7},{6,0},{7,1},{8,10},{9,11},{10,... | collective-permute-start | bytes 589832 | tf_op jit(solution)/shard_map/ppermute | solution.py:21
  124.7 12.9 %collective-permute-start.29 = (bf16[48,2048]{1,0:T(8,128)(2,1)S(1)}, bf16[48,2048]{1,0:T(8,128)(2,1)S(1)}, u32[]{:S(2)}, u32[]{:S(2)}) collective-permute-start(bf16[48,2048]{1,0:T(8,128)(2,1)S(1)} %get-tuple-element.28), channel_id=1, source_target_pairs={{0,4},{1,5},{2,6},{3,7},{4,0},{5,1},{6,2},{7,3},{8,12},{9,13},{10,... | collective-permute-start | bytes 589832 | tf_op jit(solution)/shard_map/ppermute | solution.py:21
  136.0 3.2 %collective-permute-start.30 = (bf16[144,2048]{1,0:T(8,128)(2,1)S(1)}, bf16[144,2048]{1,0:T(8,128)(2,1)S(1)}, u32[]{:S(2)}, u32[]{:S(2)}) collective-permute-start(bf16[144,2048]{1,0:T(8,128)(2,1)S(1)} %pad_maximum_fusion), channel_id=1, source_target_pairs={{0,1},{1,0},{2,3},{3,2},{4,5},{5,4},{6,7},{7,6},{8,9},{9,8},{10,11... | collective-permute-start | bytes 1769480 | tf_op jit(solution)/shard_map/ppermute | solution.py:21
  137.6 1.9 collective-permute-start.31
  142.0 8.4 %all-to-all-start = ((f32[8,1,768]{2,1,0:T(1,128)}), f32[8,1,768]{2,1,0:T(1,128)S(1)}, u32[]{:S(2)}, u32[]{:S(2)}) async-start(f32[8,1,768]{2,1,0:T(1,128)} %broadcast_in_dim.2), calls=%async_computation | async-start | bytes 49152 | tf_op jit(solution)/shard_map/all_to_all | solution.py:104
  152.1 2.7 %collective-permute-start.32 = (bf16[192,2048]{1,0:T(8,128)(2,1)S(1)}, bf16[192,2048]{1,0:T(8,128)(2,1)S(1)}, u32[]{:S(2)}, u32[]{:S(2)}) collective-permute-start(bf16[192,2048]{1,0:T(8,128)(2,1)S(1)} %convolution_convert_fusion), channel_id=1, source_target_pairs={{0,1},{1,0},{2,3},{3,2},{4,5},{5,4},{6,7},{7,6},{8,9},{9,8},{10,11... | collective-permute-start | bytes 2359304 | tf_op jit(solution)/shard_map/ppermute | solution.py:21
  156.3 7.7 %collective-permute-start.33 = (bf16[48,2048]{1,0:T(8,128)(2,1)S(1)}, bf16[48,2048]{1,0:T(8,128)(2,1)S(1)}, u32[]{:S(2)}, u32[]{:S(2)}) collective-permute-start(bf16[48,2048]{1,0:T(8,128)(2,1)S(1)} %get-tuple-element.60), channel_id=1, source_target_pairs={{0,4},{1,5},{2,6},{3,7},{4,0},{5,1},{6,2},{7,3},{8,12},{9,13},{10,... | collective-permute-start | bytes 589832 | tf_op jit(solution)/shard_map/ppermute | solution.py:21
  157.2 9.5 %collective-permute-start.34 = (bf16[48,2048]{1,0:T(8,128)(2,1)S(1)}, bf16[48,2048]{1,0:T(8,128)(2,1)S(1)}, u32[]{:S(2)}, u32[]{:S(2)}) collective-permute-start(bf16[48,2048]{1,0:T(8,128)(2,1)S(1)} %get-tuple-element.62), channel_id=1, source_target_pairs={{0,6},{1,7},{2,0},{3,1},{4,2},{5,3},{6,4},{7,5},{8,14},{9,15},{10,... | collective-permute-start | bytes 589832 | tf_op jit(solution)/shard_map/ppermute | solution.py:21
  159.1 9.8 %collective-permute-start.35 = (bf16[48,2048]{1,0:T(8,128)(2,1)S(1)}, bf16[48,2048]{1,0:T(8,128)(2,1)S(1)}, u32[]{:S(2)}, u32[]{:S(2)}) collective-permute-start(bf16[48,2048]{1,0:T(8,128)(2,1)S(1)} %get-tuple-element.61), channel_id=1, source_target_pairs={{0,2},{1,3},{2,4},{3,5},{4,6},{5,7},{6,0},{7,1},{8,10},{9,11},{10,... | collective-permute-start | bytes 589832 | tf_op jit(solution)/shard_map/ppermute | solution.py:21
  169.5 6.0 %collective-permute-start.36 = (bf16[48,2048]{1,0:T(8,128)(2,1)S(1)}, bf16[48,2048]{1,0:T(8,128)(2,1)S(1)}, u32[]{:S(2)}, u32[]{:S(2)}) collective-permute-start(bf16[48,2048]{1,0:T(8,128)(2,1)S(1)} %get-tuple-element.22), channel_id=1, source_target_pairs={{0,6},{1,7},{2,0},{3,1},{4,2},{5,3},{6,4},{7,5},{8,14},{9,15},{10,... | collective-permute-start | bytes 589832 | tf_op jit(solution)/shard_map/ppermute | solution.py:21
  170.5 8.2 %collective-permute-start.37 = (bf16[48,2048]{1,0:T(8,128)(2,1)S(1)}, bf16[48,2048]{1,0:T(8,128)(2,1)S(1)}, u32[]{:S(2)}, u32[]{:S(2)}) collective-permute-start(bf16[48,2048]{1,0:T(8,128)(2,1)S(1)} %get-tuple-element.22), channel_id=1, source_target_pairs={{0,2},{1,3},{2,4},{3,5},{4,6},{5,7},{6,0},{7,1},{8,10},{9,11},{10,... | collective-permute-start | bytes 589832 | tf_op jit(solution)/shard_map/ppermute | solution.py:21
  171.0 12.4 %collective-permute-start.38 = (bf16[48,2048]{1,0:T(8,128)(2,1)S(1)}, bf16[48,2048]{1,0:T(8,128)(2,1)S(1)}, u32[]{:S(2)}, u32[]{:S(2)}) collective-permute-start(bf16[48,2048]{1,0:T(8,128)(2,1)S(1)} %get-tuple-element.22), channel_id=1, source_target_pairs={{0,4},{1,5},{2,6},{3,7},{4,0},{5,1},{6,2},{7,3},{8,12},{9,13},{10,... | collective-permute-start | bytes 589832 | tf_op jit(solution)/shard_map/ppermute | solution.py:21
  178.8 6.2 %collective-permute-start.39 = (bf16[144,2048]{1,0:T(8,128)(2,1)S(1)}, bf16[144,2048]{1,0:T(8,128)(2,1)S(1)}, u32[]{:S(2)}, u32[]{:S(2)}) collective-permute-start(bf16[144,2048]{1,0:T(8,128)(2,1)S(1)} %pad_maximum_fusion.1), channel_id=1, source_target_pairs={{0,1},{1,0},{2,3},{3,2},{4,5},{5,4},{6,7},{7,6},{8,9},{9,8},{10,11... | collective-permute-start | bytes 1769480 | tf_op jit(solution)/shard_map/ppermute | solution.py:21
  183.4 1.9 collective-permute-start.40
  193.3 2.4 %collective-permute-start.41 = (bf16[192,2048]{1,0:T(8,128)(2,1)S(1)}, bf16[192,2048]{1,0:T(8,128)(2,1)S(1)}, u32[]{:S(2)}, u32[]{:S(2)}) collective-permute-start(bf16[192,2048]{1,0:T(8,128)(2,1)S(1)} %fusion.15), channel_id=1, source_target_pairs={{0,1},{1,0},{2,3},{3,2},{4,5},{5,4},{6,7},{7,6},{8,9},{9,8},{10,11... | collective-permute-start | bytes 2359304 | tf_op jit(solution)/shard_map/ppermute | solution.py:21
  196.6 7.7 %collective-permute-start.42 = (bf16[48,2048]{1,0:T(8,128)(2,1)S(1)}, bf16[48,2048]{1,0:T(8,128)(2,1)S(1)}, u32[]{:S(2)}, u32[]{:S(2)}) collective-permute-start(bf16[48,2048]{1,0:T(8,128)(2,1)S(1)} %get-tuple-element.57), channel_id=1, source_target_pairs={{0,4},{1,5},{2,6},{3,7},{4,0},{5,1},{6,2},{7,3},{8,12},{9,13},{10,... | collective-permute-start | bytes 589832 | tf_op jit(solution)/shard_map/ppermute | solution.py:21
  196.6 8.7 %collective-permute-start.43 = (bf16[48,2048]{1,0:T(8,128)(2,1)S(1)}, bf16[48,2048]{1,0:T(8,128)(2,1)S(1)}, u32[]{:S(2)}, u32[]{:S(2)}) collective-permute-start(bf16[48,2048]{1,0:T(8,128)(2,1)S(1)} %get-tuple-element.59), channel_id=1, source_target_pairs={{0,6},{1,7},{2,0},{3,1},{4,2},{5,3},{6,4},{7,5},{8,14},{9,15},{10,... | collective-permute-start | bytes 589832 | tf_op jit(solution)/shard_map/ppermute | solution.py:21
  196.7 12.4 %collective-permute-start.44 = (bf16[48,2048]{1,0:T(8,128)(2,1)S(1)}, bf16[48,2048]{1,0:T(8,128)(2,1)S(1)}, u32[]{:S(2)}, u32[]{:S(2)}) collective-permute-start(bf16[48,2048]{1,0:T(8,128)(2,1)S(1)} %get-tuple-element.58), channel_id=1, source_target_pairs={{0,2},{1,3},{2,4},{3,5},{4,6},{5,7},{6,0},{7,1},{8,10},{9,11},{10,... | collective-permute-start | bytes 589832 | tf_op jit(solution)/shard_map/ppermute | solution.py:21
  (13 other events, 72.9 us)
Sparse Core Ops, SparseCore 0:
  10.2 75.0 all-gather.2
  87.4 85.7 all-gather.4
